TPU v7x, 256 devices: a 4x2x16 block of a 4x16x16 slice. The times are simulated.
256 devices in a mesh: grp: 2 (over y), sp: 32 (over z, core), tp: 4 (over x).
Axes of the slice: x: 4, y: 2, z: 16, core: 2. Of those that a mesh axis runs over, the one named last changes fastest.
The devices are a block of a 4x16x16 slice.
Arguments:
- queries: bfloat16 [16384, 512], P(('grp', 'sp'), 'tp'), parts along dimension 0, may hold values from -6 to 6
- key_rows: bfloat16 [16384, 512], P(('grp', 'sp'), 'tp'), parts along dimension 0, may hold values from -6 to 6
- value_rows: bfloat16 [16384, 1024], P(('grp', 'sp'), 'tp'), parts along dimension 0, may hold values from -6 to 6
- out_gate: bfloat16 [16384, 1024], P(('grp', 'sp'), 'tp'), parts along dimension 0, may hold values from -6 to 6
- log_decay: float32 [2, 16384, 512], P(None, ('grp', 'sp'), 'tp'), parts along dimension 1
- doc_ids: int32 [16384], P(('grp', 'sp')), parts along dimension 0, may hold values from 0 to 3, as said below
- head_gain: float32 [1024], P('tp'), may hold values from 0.1 to 1.9
- out_weight: bfloat16 [1024, 2048], P('tp'), may hold values from -0.375 to 0.375
- residual: bfloat16 [16384, 2048], P(('grp', 'sp'), 'tp'), parts along dimension 0
- norm_gain: float32 [2, 2048], replicated, may hold values from 0.1 to 1.9
- norm_bias: float32 [2, 2048], replicated, may hold values from -3 to 3
- gate_weight: bfloat16 [2048, 3072], P('sp', 'tp'), may hold values from -0.125 to 0.125
- up_weight: bfloat16 [2048, 3072], P('sp', 'tp'), may hold values from -0.125 to 0.125
- down_weight: bfloat16 [3072, 2048], P('tp', 'sp'), may hold values from -0.109375 to 0.109375
Outputs:
- layer_out: bfloat16 [16384, 2048], P(('grp', 'sp'), 'tp'), parts along dimension 0
There are 2 independent parts, one for each index of `grp`. A program takes and returns all parts, laid end to end along the dimension named above; an argument that names none is the same for every part. Nothing has to cross between parts.
Inputs may be any that keep to these rules, and one draw needn't show every extreme that they name: `doc_ids`: document numbers start at 0 and never fall; they rise by one at each of 3 positions, the k-th rise lying within half of 256 positions of k times 8192 divided by 4.
All inputs are finite; a program needn't handle non-finite values.
Results may differ from a plain program's by a relative error of at most 0.009.
Values may be sent and summed in bfloat16 or wider, within the bound.
No kernel may reach another device: no remote copies, remote signals or barrier semaphores. Data moves between devices by JAX's collectives and lax.ppermute only.
A program may use at most 128 MiB of HBM per device.

v0:
```python
import jax
import jax.numpy as jnp
from jax import lax
from jax.sharding import PartitionSpec as P

DK = 32
DV = 64
BLOCK = 64


EPS = 1e-06
HIGH = lax.Precision.HIGHEST


def sent_to_all(x, axis):
    peers = lax.axis_size(axis)
    return lax.all_to_all(jnp.broadcast_to(x[None], (peers, *x.shape)), axis, 0, 0, tiled=True)


def all_in_one(x, axis):
    leaves = jax.tree.leaves(x)
    turns = sorted(range(len(leaves)), key=lambda k: -leaves[k].size)
    width = (1, *leaves[turns[0]].shape)[-1]
    lines = [
        jnp.pad(leaves[k].reshape(-1), (0, -leaves[k].size % width)).reshape(-1, width)
        for k in turns
    ]
    both, at, found = (sent_to_all(jnp.concatenate(lines), axis), 0, {})
    for k, line in zip(turns, lines):
        piece = both[:, at : at + len(line)].reshape(len(both), -1)
        found[k] = piece[:, : leaves[k].size].reshape(-1, *leaves[k].shape)
        at += len(line)
    numbers = iter(range(len(leaves)))
    return jax.tree.map(lambda _: found[next(numbers)], x)


def folded_in_pairs(pieces, combine):
    while len(jax.tree.leaves(pieces)[0]) > 1:
        pieces = jax.vmap(combine)(
            *(jax.tree.map(lambda part: part[side::2], pieces) for side in (0, 1))
        )
    return jax.tree.map(lambda part: part[0], pieces)


def prefix(x, axis, combine, identity, reverse):
    peers, position = (lax.axis_size(axis), lax.axis_index(axis))
    passed = jnp.arange(peers) > position if reverse else jnp.arange(peers) < position

    def kept(part, zero, own):
        part = jnp.where(
            passed.reshape(-1, *(1 for _ in own.shape)),
            part.astype(own.dtype),
            jnp.asarray(zero, own.dtype),
        )
        return part[::-1] if reverse else part

    pieces = all_in_one(
        jax.tree.map(
            lambda part, kind: part.astype(kind),
            x,
            jax.tree.map(lambda a: jnp.bfloat16 if a.dtype == jnp.float32 else a.dtype, x),
        ),
        axis,
    )
    return folded_in_pairs(jax.tree.map(kept, pieces, identity, x), combine)


def rows_first(arrays, axis, dims):
    turned = [jnp.moveaxis(a, dim, 0) for a, dim in zip(arrays, dims)]
    both = jnp.concatenate([t.reshape(len(t), -1) for t in turned], axis=1)
    result, at, gathered = (lax.all_gather(both, axis, axis=0, tiled=True), 0, [])
    for t, dim in zip(turned, dims):
        piece = result[:, at : at + t[0].size].reshape(-1, *t.shape[1:])
        gathered.append(jnp.moveaxis(piece, 0, dim))
        at += t[0].size
    return tuple(gathered)


def cut_along(x, dim, peers):
    shape = x.shape
    parts = x.reshape(*shape[:dim], peers, shape[dim] // peers, *shape[dim + 1 :])
    return jnp.moveaxis(parts, dim, 0)


def summed_on_arrival(x, axis, dim):
    peers = lax.axis_size(axis)
    parts = lax.all_to_all(cut_along(x, dim, peers), axis, 0, 0, tiled=True)
    return jnp.sum(parts.astype(jnp.float32), axis=0)


def over_copies(x, axis):
    everything = sent_to_all(x, axis)
    return jnp.sum(everything, axis=0)


def together(arrays, axis):
    ravelled, at, gathered = (jnp.concatenate([a.reshape(-1) for a in arrays]), 0, [])
    total = over_copies(ravelled, axis)
    for a in arrays:
        gathered.append(total[at : at + a.size].reshape(a.shape))
        at += a.size
    return tuple(gathered)


def in_order(parts, dim):
    parts = jnp.moveaxis(parts, 0, dim)
    shape = parts.shape
    return parts.reshape(*shape[:dim], shape[dim] * shape[dim + 1], *shape[dim + 2 :])


def gather_directly(x, axis, dim):
    return in_order(sent_to_all(x, axis), dim)


def run_blocks(query, key_part, value_part, decay, docs):
    length = query.shape[0]
    count = length // BLOCK
    head_count = query.shape[1]
    lower = jnp.arange(BLOCK)[:, None] >= jnp.arange(BLOCK)[None, :]

    def blocked(array):
        return array.reshape((count, BLOCK) + array.shape[1:])

    def advance(carried, inputs):
        state, state_doc = carried
        query_block, key_block, value_block, decay_block, doc_block = inputs
        running = jnp.cumsum(decay_block, axis=0)
        allowed = lower & (doc_block[:, None] == doc_block[None, :])
        relative = jnp.exp(
            jnp.where(allowed[:, :, None, None], running[:, None] - running[None, :], -jnp.inf)
        )
        scores = jnp.einsum("ihd,jhd,ijhd->hij", query_block, key_block, relative, precision=HIGH)
        within = jnp.einsum("hij,jhe->ihe", scores, value_block, precision=HIGH)
        linked = (doc_block == state_doc).astype(jnp.float32)
        carried_part = (
            jnp.einsum("ihd,hde->ihe", query_block * jnp.exp(running), state, precision=HIGH)
            * linked[:, None, None]
        )
        closing = doc_block[-1]
        ending = (doc_block == closing).astype(jnp.float32)
        tail_decay = jnp.exp(running[-1][None] - running) * ending[:, None, None]
        kept = (state_doc == closing).astype(jnp.float32)
        state = kept * jnp.exp(running[-1])[:, :, None] * state + jnp.einsum(
            "jhd,jhe->hde", key_block * tail_decay, value_block, precision=HIGH
        )
        return ((state, closing), within + carried_part)

    start = (
        jnp.zeros((head_count, query.shape[2], value_part.shape[2]), jnp.float32),
        jnp.array(-1, jnp.int32),
    )
    (state, closing), outputs = lax.scan(
        advance,
        start,
        tuple((blocked(array) for array in (query, key_part, value_part, decay, docs))),
    )
    return (outputs.reshape(length, head_count, value_part.shape[2]), state, closing)


def chain(earlier, later):
    early_state, early_pass, early_entry, early_leave = earlier
    late_state, late_pass, late_entry, late_leave = later
    joined = (late_entry == early_leave) | (early_leave < 0.0) | (late_entry < 0.0)
    keep = jnp.where(joined, jnp.float32(1.0), jnp.float32(0.0))
    state = late_state + keep * late_pass[:, :, None] * early_state
    passing = keep * early_pass * late_pass
    entry = jnp.where(early_entry < 0.0, late_entry, early_entry)
    leaving = jnp.where(late_leave < 0.0, early_leave, late_leave)
    return (state, passing, entry, leaving)


def one_way(query, key_part, value_part, decay, docs, backward):
    local_out, state, closing = run_blocks(query, key_part, value_part, decay, docs)
    passing = jnp.exp(jnp.sum(decay, axis=0)) * (docs[0] == closing).astype(jnp.float32)
    piece = (state, passing, docs[0].astype(jnp.float32), closing.astype(jnp.float32))
    identity = (jnp.zeros_like(state), jnp.ones_like(passing), jnp.float32(-1.0), jnp.float32(-1.0))
    if backward:
        carried = prefix(piece, "sp", chain, identity, True)
    else:
        carried = prefix(piece, "sp", chain, identity, False)
    incoming, _, _, leaving = carried
    linked = (docs.astype(jnp.float32) == leaving).astype(jnp.float32)
    reach = query * jnp.exp(jnp.cumsum(decay, axis=0))
    return (
        local_out
        + jnp.einsum("ihd,hde->ihe", reach, incoming, precision=HIGH) * linked[:, None, None]
    )


def apply_norm(stream, moments, full_width, gain, bias):
    middle = moments[0][:, None] / full_width
    spread = moments[1][:, None] / full_width - middle * middle
    return (stream - middle) * lax.rsqrt(spread + EPS) * gain + bias


def on_device(
    queries,
    key_rows,
    value_rows,
    out_gate,
    log_decay,
    doc_ids,
    head_gain,
    out_weight,
    residual,
    norm_gain,
    norm_bias,
    gate_weight,
    up_weight,
    down_weight,
):
    collected = None
    length = queries.shape[0]
    head_count = queries.shape[1] // DK
    query = queries.astype(jnp.float32).reshape(length, head_count, DK) * DK ** (-0.5)
    key_part = key_rows.astype(jnp.float32).reshape(length, head_count, DK)
    value_part = value_rows.astype(jnp.float32).reshape(length, head_count, DV)
    forward_decay = log_decay[0].reshape(length, head_count, DK)
    backward_decay = log_decay[1].reshape(length, head_count, DK)
    forward_out = one_way(query, key_part, value_part, forward_decay, doc_ids, False)
    backward_out = one_way(
        query[::-1], key_part[::-1], value_part[::-1], backward_decay[::-1], doc_ids[::-1], True
    )[::-1]
    attended = forward_out + backward_out
    normed = attended * lax.rsqrt(jnp.mean(attended * attended, axis=-1, keepdims=True) + EPS)
    mixed = (
        normed.reshape(length, -1) * head_gain * jax.nn.silu(out_gate.astype(jnp.float32))
    ).astype(jnp.bfloat16)
    partial_value = jnp.dot(mixed, out_weight, preferred_element_type=jnp.float32)
    collected = rows_first((gate_weight, up_weight, down_weight), "sp", (0, 0, 1))
    gate_full, up_full, down_full = collected
    own_width = residual.shape[1]
    full_width = own_width * lax.axis_size("tp")
    offset = lax.axis_index("tp") * own_width
    branch = summed_on_arrival(partial_value.astype(jnp.bfloat16), "tp", 1)
    stream = residual.astype(jnp.float32) + branch
    moments = together((jnp.sum(stream, axis=1), jnp.sum(stream * stream, axis=1)), "tp")
    settled = apply_norm(
        stream,
        moments,
        full_width,
        lax.dynamic_slice_in_dim(norm_gain[0], offset, own_width, 0),
        lax.dynamic_slice_in_dim(norm_bias[0], offset, own_width, 0),
    )
    features = settled.astype(jnp.bfloat16)
    piece = gather_directly(features, "tp", 1)
    gate = jnp.dot(piece, gate_full, preferred_element_type=jnp.float32)
    up_part = jnp.dot(piece, up_full, preferred_element_type=jnp.float32)
    inner = (jax.nn.silu(gate) * up_part).astype(jnp.bfloat16)
    down = summed_on_arrival(
        jnp.dot(inner, down_full, preferred_element_type=jnp.float32).astype(jnp.bfloat16), "tp", 1
    )
    final = settled + 0.5 * down
    closing_moments = together((jnp.sum(final, axis=1), jnp.sum(final * final, axis=1)), "tp")
    result = apply_norm(
        final,
        closing_moments,
        full_width,
        lax.dynamic_slice_in_dim(norm_gain[1], offset, own_width, 0),
        lax.dynamic_slice_in_dim(norm_bias[1], offset, own_width, 0),
    )
    return result.astype(jnp.bfloat16)


def solution(mesh):
    in_specs = (
        P(("grp", "sp"), "tp"),
        P(("grp", "sp"), "tp"),
        P(("grp", "sp"), "tp"),
        P(("grp", "sp"), "tp"),
        P(None, ("grp", "sp"), "tp"),
        P(("grp", "sp")),
        P("tp"),
        P("tp", None),
        P(("grp", "sp"), "tp"),
        P(),
        P(),
        P("sp", "tp"),
        P("sp", "tp"),
        P("tp", "sp"),
    )
    out_specs = P(("grp", "sp"), "tp")
    return jax.shard_map(
        on_device, mesh=mesh, in_specs=in_specs, out_specs=out_specs, check_vma=False
    )
```

profile of v0, /device:TPU:40, one launch (start us, length us, event | category | flops | bytes accessed | tf_op | source)
XLA Modules:
  0.0 438.3 jit_solution(17163020052627805897)
XLA Ops:
  15.0 81.2 %while.30 = (s32[]{:T(128)}, f32[4,32,64]{2,1,0:T(8,128)S(1)}, s32[]{:T(128)}, f32[4,64,4,64]{1,0,3,2:T(4,128)S(1)}, s32[4,64]{1,0:T(4,128)S(1)}, /*index=5*/f32...) while((s32[]{:T(128)}, f32[4,32,64]{2,1,0:T(8,128)S(1)}, ...), condition=%wide.region_2.3_spmd.clone, body=%wide.region_0.2_spmd.clone.sunk | while | flops 28397956 | bytes 10237110 | solution.py:152
  18.5 3.2 exponential_bitcast_fusion.10
  21.7 5.9 %copy.513 = f32[4,64,64,32]{1,2,3,0:T(8,128)} copy(f32[4,64,64,32]{2,3,0,1:T(8,128)} %exponential_bitcast_fusion.10) | data formatting | bytes 4194304 | tf_op jit(solution)/shard_map/while
  27.7 2.9 fusion.154
  31.0 2.8 dynamic_update_slice.11
  38.8 3.2 exponential_bitcast_fusion.10
  42.0 5.9 %copy.513 = f32[4,64,64,32]{1,2,3,0:T(8,128)} copy(f32[4,64,64,32]{2,3,0,1:T(8,128)} %exponential_bitcast_fusion.10) | data formatting | bytes 4194304 | tf_op jit(solution)/shard_map/while
  48.0 2.9 fusion.154
  59.1 3.2 exponential_bitcast_fusion.10
  62.3 5.9 %copy.513 = f32[4,64,64,32]{1,2,3,0:T(8,128)} copy(f32[4,64,64,32]{2,3,0,1:T(8,128)} %exponential_bitcast_fusion.10) | data formatting | bytes 4194304 | tf_op jit(solution)/shard_map/while
  68.3 2.9 fusion.154
  71.6 2.8 dynamic_update_slice.11
  79.4 3.2 exponential_bitcast_fusion.10
  82.6 5.9 %copy.513 = f32[4,64,64,32]{1,2,3,0:T(8,128)} copy(f32[4,64,64,32]{2,3,0,1:T(8,128)} %exponential_bitcast_fusion.10) | data formatting | bytes 4194304 | tf_op jit(solution)/shard_map/while
  88.6 2.9 fusion.154
  91.9 2.8 dynamic_update_slice.11
  99.5 24.7 %all-to-all-start = ((bf16[32,132,64]{1,2,0:T(8,128)(2,1)}), bf16[32,132,64]{1,2,0:T(8,128)(2,1)S(1)}, u32[]{:S(2)}, u32[]{:S(2)}) async-start(bf16[32,132,64]{1,2,0:T(8,128)(2,1)} %broadcast_in_dim.135), calls=%async_computation | async-start | bytes 2097152 | tf_op jit(solution)/shard_map/all_to_all | solution.py:17
  133.7 97.2 %while.31 = (s32[]{:T(128)}, f32[4,32,64]{2,1,0:T(8,128)S(1)}, s32[]{:T(128)}, f32[4,64,4,64]{1,0,3,2:T(4,128)}, s32[4,64]{1,0:T(4,128)S(1)}, /*index=5*/f32[4,6...) while((s32[]{:T(128)}, f32[4,32,64]{2,1,0:T(8,128)S(1)}, ...), condition=%wide.region_8.9_spmd.clone, body=%wide.region_6.8_spmd.clone.sunk | while | flops 28397956 | bytes 10073782 | solution.py:152
  134.9 3.2 exponential_bitcast_fusion.11
  138.1 5.8 %copy.519 = f32[4,64,64,32]{1,2,3,0:T(8,128)} copy(f32[4,64,64,32]{2,3,0,1:T(8,128)} %exponential_bitcast_fusion.11) | data formatting | bytes 4194304 | tf_op jit(solution)/shard_map/while
  145.0 2.9 fusion.166
  151.9 4.5 %dynamic_update_slice.12 = f32[4,64,4,64]{1,0,3,2:T(4,128)} dynamic-update-slice(f32[4,64,4,64]{1,0,3,2:T(4,128)} %get-tuple-element.589, f32[1,64,4,64]{1,0,3,2:T(1,128)S(1)} %bitcast.312, s32[]{:T(128)} %get-tuple-element.586, s32[]{:T(128)} %constant.83.clone.1..sunk.1, s32[]{:T(128)} %constant.83.clone.1..sunk.1, s32[]{:T(128)} %constant.83.clone.1..sunk.1) | dynamic-update-slice | bytes 131076 | tf_op jit(solution)/shard_map/while/body/jit(dynamic_update_index_in_dim)/dynamic_update_slice | solution.py:152
  159.1 3.2 exponential_bitcast_fusion.11
  162.3 5.8 %copy.519 = f32[4,64,64,32]{1,2,3,0:T(8,128)} copy(f32[4,64,64,32]{2,3,0,1:T(8,128)} %exponential_bitcast_fusion.11) | data formatting | bytes 4194304 | tf_op jit(solution)/shard_map/while
  169.3 2.9 fusion.166
  176.2 4.5 %dynamic_update_slice.12 = f32[4,64,4,64]{1,0,3,2:T(4,128)} dynamic-update-slice(f32[4,64,4,64]{1,0,3,2:T(4,128)} %get-tuple-element.589, f32[1,64,4,64]{1,0,3,2:T(1,128)S(1)} %bitcast.312, s32[]{:T(128)} %get-tuple-element.586, s32[]{:T(128)} %constant.83.clone.1..sunk.1, s32[]{:T(128)} %constant.83.clone.1..sunk.1, s32[]{:T(128)} %constant.83.clone.1..sunk.1) | dynamic-update-slice | bytes 131076 | tf_op jit(solution)/shard_map/while/body/jit(dynamic_update_index_in_dim)/dynamic_update_slice | solution.py:152
  183.3 3.2 exponential_bitcast_fusion.11
  186.6 5.8 %copy.519 = f32[4,64,64,32]{1,2,3,0:T(8,128)} copy(f32[4,64,64,32]{2,3,0,1:T(8,128)} %exponential_bitcast_fusion.11) | data formatting | bytes 4194304 | tf_op jit(solution)/shard_map/while
  193.5 3.0 fusion.166
  200.5 4.5 %dynamic_update_slice.12 = f32[4,64,4,64]{1,0,3,2:T(4,128)} dynamic-update-slice(f32[4,64,4,64]{1,0,3,2:T(4,128)} %get-tuple-element.589, f32[1,64,4,64]{1,0,3,2:T(1,128)S(1)} %bitcast.312, s32[]{:T(128)} %get-tuple-element.586, s32[]{:T(128)} %constant.83.clone.1..sunk.1, s32[]{:T(128)} %constant.83.clone.1..sunk.1, s32[]{:T(128)} %constant.83.clone.1..sunk.1) | dynamic-update-slice | bytes 131076 | tf_op jit(solution)/shard_map/while/body/jit(dynamic_update_index_in_dim)/dynamic_update_slice | solution.py:152
  207.7 3.2 exponential_bitcast_fusion.11
  210.9 5.9 %copy.519 = f32[4,64,64,32]{1,2,3,0:T(8,128)} copy(f32[4,64,64,32]{2,3,0,1:T(8,128)} %exponential_bitcast_fusion.11) | data formatting | bytes 4194304 | tf_op jit(solution)/shard_map/while
  217.9 3.0 fusion.166
  224.9 4.5 %dynamic_update_slice.12 = f32[4,64,4,64]{1,0,3,2:T(4,128)} dynamic-update-slice(f32[4,64,4,64]{1,0,3,2:T(4,128)} %get-tuple-element.589, f32[1,64,4,64]{1,0,3,2:T(1,128)S(1)} %bitcast.312, s32[]{:T(128)} %get-tuple-element.586, s32[]{:T(128)} %constant.83.clone.1..sunk.1, s32[]{:T(128)} %constant.83.clone.1..sunk.1, s32[]{:T(128)} %constant.83.clone.1..sunk.1) | dynamic-update-slice | bytes 131076 | tf_op jit(solution)/shard_map/while/body/jit(dynamic_update_index_in_dim)/dynamic_update_slice | solution.py:152
  235.9 4.3 reduce-window.16
  240.2 4.3 reduce-window.14
  246.6 12.7 %all-to-all-start.1 = ((bf16[32,132,64]{1,2,0:T(8,128)(2,1)}), bf16[32,132,64]{1,2,0:T(8,128)(2,1)}, u32[]{:S(2)}, u32[]{:S(2)}) async-start(bf16[32,132,64]{1,2,0:T(8,128)(2,1)} %broadcast_in_dim.209), calls=%async_computation.1 | async-start | bytes 2097152 | tf_op jit(solution)/shard_map/all_to_all | solution.py:17
  270.3 44.1 %all-to-all-done.1 = bf16[32,132,64]{1,2,0:T(8,128)(2,1)} async-done(((bf16[32,132,64]{1,2,0:T(8,128)(2,1)}), bf16[32,132,64]{1,2,0:T(8,128)(2,1)}, u32[]{:S(2)}, u32[]{:S(2)}) %all-to-all-start.1) | async-done | bytes 540704 | tf_op jit(solution)/shard_map/all_to_all | solution.py:17
  349.4 4.6 %all-to-all-start.2 = ((bf16[4,256,512]{2,1,0:T(8,128)(2,1)}), bf16[4,256,512]{2,1,0:T(8,128)(2,1)S(1)}, u32[]{:S(2)}, u32[]{:S(2)}) async-start(bf16[4,256,512]{2,1,0:T(8,128)(2,1)} %bitcast.317), calls=%async_computation.2 | async-start | bytes 2097152 | tf_op jit(solution)/shard_map/all_to_all | solution.py:87
  354.1 15.2 %all-to-all-done.2 = bf16[4,256,512]{2,1,0:T(8,128)(2,1)S(1)} async-done(((bf16[4,256,512]{2,1,0:T(8,128)(2,1)}), bf16[4,256,512]{2,1,0:T(8,128)(2,1)S(1)}, u32[]{:S(2)}, u32[]{:S(2)}) %all-to-all-start.2) | async-done | bytes 1048608 | tf_op jit(solution)/shard_map/all_to_all | solution.py:87
  370.2 3.3 all-to-all-start.3
  373.6 5.2 %all-to-all-done.3 = f32[4,1,512]{2,1,0:T(1,128)S(1)} async-done(((f32[4,1,512]{2,1,0:T(1,128)}), f32[4,1,512]{2,1,0:T(1,128)S(1)}, u32[]{:S(2)}, u32[]{:S(2)}) %all-to-all-start.3) | async-done | bytes 8224 | tf_op jit(solution)/shard_map/all_to_all | solution.py:17
  379.2 15.7 %all_to_all.37 = bf16[4,256,512]{1,2,0:T(8,128)(2,1)S(1)} all-to-all(bf16[4,256,512]{1,2,0:T(8,128)(2,1)S(1)} %broadcast_in_dim.212), channel_id=1, replica_groups=mesh['grp'=2,'sp'=32,'tp'=4] {'tp'}, dimensions={0} | all-to-all | bytes 2097152 | tf_op jit(solution)/shard_map/all_to_all | solution.py:17
  394.9 3.8 fusion.34
  398.7 6.3 %fusion.36 = bf16[256,2048]{1,0:T(8,128)(2,1)} fusion(bf16[2048,2304]{1,0:T(8,128)(2,1)} %all-gather.2.cloned.1.call-done, bf16[256,2048]{0,1:T(8,128)(2,1)S(1)} %bitcast.323, f32[256,768]{1,0:T(8,128)} %fusion.34), kind=kOutput, calls=%fused_computation.68 | convolution fusion | flops 1612316672 | bytes 9175040 | tf_op jit(solution)/shard_map/dot_general | solution.py:251
  406.3 14.5 %all_to_all.38 = bf16[4,256,512]{2,1,0:T(8,128)(2,1)S(1)} all-to-all(bf16[4,256,512]{2,1,0:T(8,128)(2,1)S(1)} %bitcast.318), channel_id=1, replica_groups=mesh['grp'=2,'sp'=32,'tp'=4] {'tp'}, dimensions={0} | all-to-all | bytes 2097152 | tf_op jit(solution)/shard_map/all_to_all | solution.py:87
  422.0 3.3 all-to-all-start.6
  425.3 5.2 %all-to-all-done.6 = f32[4,1,512]{2,1,0:T(1,128)S(1)} async-done(((f32[4,1,512]{2,1,0:T(1,128)}), f32[4,1,512]{2,1,0:T(1,128)S(1)}, u32[]{:S(2)}, u32[]{:S(2)}) %all-to-all-start.6) | async-done | bytes 8224 | tf_op jit(solution)/shard_map/all_to_all | solution.py:17
  (407 shorter events, 112.9 us)
Async XLA Ops:
  6.5 341.2 %copy-start = (bf16[256,2048]{1,0:T(8,128)(2,1)S(1)}, bf16[256,2048]{1,0:T(8,128)(2,1)}, u32[]{:S(2)}) copy-start(bf16[256,2048]{1,0:T(8,128)(2,1)} %param.25) | copy-start | bytes 3145732
  10.5 4.5 %copy-start.7 = (f32[1,256,128]{1,2,0:T(8,128)}, f32[1,256,128]{1,2,0:T(8,128)S(1)}, u32[]{:S(2)}) copy-start(f32[1,256,128]{1,2,0:T(8,128)S(1)} %copy.431) | copy-start | bytes 393220
  11.7 3.2 copy-start.5
  14.1 0.9 copy-start.14
  96.2 3.2 copy-start.2
  96.2 30.0 %copy-start.6 = (bf16[256,256]{0,1:T(8,128)(2,1)S(1)}, bf16[256,256]{0,1:T(8,128)(2,1)}, u32[]{:S(2)}) copy-start(bf16[256,256]{0,1:T(8,128)(2,1)} %copy-done.5) | copy-start | bytes 393220
  96.2 30.1 %copy-start.15 = (bf16[256,128]{0,1:T(8,128)(2,1)S(1)}, bf16[256,128]{0,1:T(8,128)(2,1)}, u32[]{:S(2)}) copy-start(bf16[256,128]{0,1:T(8,128)(2,1)} %copy-done.14) | copy-start | bytes 196612
  96.2 30.7 %copy-start.19 = (s32[256]{0:T(256)S(1)}, s32[256]{0:T(256)}, u32[]{:S(2)}) copy-start(s32[256]{0:T(256)} %param.23) | copy-start | bytes 3076
  96.3 30.8 %copy-start.16 = (f32[1,256,128]{2,1,0:T(8,128)S(1)}, f32[1,256,128]{2,1,0:T(8,128)}, u32[]{:S(2)}) copy-start(f32[1,256,128]{2,1,0:T(8,128)} %get-tuple-element.370) | copy-start | bytes 393220
  99.5 146.1 %all-to-all-start = ((bf16[32,132,64]{1,2,0:T(8,128)(2,1)}), bf16[32,132,64]{1,2,0:T(8,128)(2,1)S(1)}, u32[]{:S(2)}, u32[]{:S(2)}) async-start(bf16[32,132,64]{1,2,0:T(8,128)(2,1)} %broadcast_in_dim.135), calls=%async_computation | async-start | bytes 2097152 | tf_op jit(solution)/shard_map/all_to_all | solution.py:17
  124.2 270.7 %all-gather.2.cloned.1.call-start = ((), (), s32[]{:S(2)}) async-start(), calls=%async_computation.7 | async-start | bytes 9732096 | tf_op jit(solution)/shard_map/all_gather | solution.py:71
  127.1 6.6 %copy-start.23 = (s32[256]{0:T(256)}, s32[256]{0:T(256)S(1)}, u32[]{:S(2)}) copy-start(s32[256]{0:T(256)S(1)} %rev.22) | copy-start | bytes 3076
  128.5 0.6 copy-start.8
  230.9 28.6 %copy-start.4 = (f32[4,64,4,64]{1,0,3,2:T(4,128)S(1)}, f32[4,64,4,64]{1,0,3,2:T(4,128)}, u32[]{:S(2)}) copy-start(f32[4,64,4,64]{1,0,3,2:T(4,128)} %get-tuple-element.116) | copy-start | bytes 786436
  230.9 29.6 %copy-start.3 = (f32[4,64,4,64]{1,0,3,2:T(4,128)S(1)}, f32[4,64,4,64]{1,0,3,2:T(4,128)}, u32[]{:S(2)}) copy-start(f32[4,64,4,64]{1,0,3,2:T(4,128)} %copy-done.2) | copy-start | bytes 786436
  240.2 22.9 %copy-start.10 = (f32[32,4,2,128]{3,0,1,2:T(8,128)}, f32[32,4,2,128]{3,0,1,2:T(8,128)S(1)}, u32[]{:S(2)}) copy-start(f32[32,4,2,128]{3,0,1,2:T(8,128)S(1)} %reduce-window.16) | copy-start | bytes 393220
  245.5 70.6 %copy-start.17 = (f32[32,4,3]{0,1,2:T(4,128)}, f32[32,4,3]{0,1,2:T(4,128)S(1)}, u32[]{:S(2)}) copy-start(f32[32,4,3]{0,1,2:T(4,128)S(1)} %fusion.107) | copy-start | bytes 4612
  246.6 67.8 %all-to-all-start.1 = ((bf16[32,132,64]{1,2,0:T(8,128)(2,1)}), bf16[32,132,64]{1,2,0:T(8,128)(2,1)}, u32[]{:S(2)}, u32[]{:S(2)}) async-start(bf16[32,132,64]{1,2,0:T(8,128)(2,1)} %broadcast_in_dim.209), calls=%async_computation.1 | async-start | bytes 2097152 | tf_op jit(solution)/shard_map/all_to_all | solution.py:17
  261.6 64.0 %copy-start.18 = (f32[32,4,3]{0,1,2:T(4,128)}, f32[32,4,3]{0,1,2:T(4,128)S(1)}, u32[]{:S(2)}) copy-start(f32[32,4,3]{0,1,2:T(4,128)S(1)} %fusion.106) | copy-start | bytes 4612
  266.6 58.9 %copy-start.28 = (f32[2]{0:T(128)}, f32[2]{0:T(128)S(1)}, u32[]{:S(2)}) copy-start(f32[2]{0:T(128)S(1)} %get-tuple-element.402) | copy-start | bytes 28
  324.4 11.9 %copy-start.24 = (s32[256]{0:T(256)S(1)}, s32[256]{0:T(256)}, u32[]{:S(2)}) copy-start(s32[256]{0:T(256)} %copy-done.23) | copy-start | bytes 3076
  340.7 1.2 copy-start.9
  340.8 1.2 copy-start.11
  340.8 1.2 copy-start.13
  340.8 1.2 slice-start
  341.1 1.8 copy-start.20
  341.1 2.5 copy-start.25
  341.1 2.6 copy-start.26
  341.1 2.7 copy-start.27
  345.2 1.7 copy-start.12
  345.2 1.7 slice-start.1
  346.1 1.7 copy-start.29
  346.1 1.7 copy-start.30
  347.0 7.0 %copy-start.21 = (f32[2,2048]{1,0:T(2,128)S(1)}, f32[2,2048]{1,0:T(2,128)}, u32[]{:S(2)}) copy-start(f32[2,2048]{1,0:T(2,128)} %param.27) | copy-start | bytes 49156
  347.6 6.4 %copy-start.22 = (f32[2,2048]{1,0:T(2,128)S(1)}, f32[2,2048]{1,0:T(2,128)}, u32[]{:S(2)}) copy-start(f32[2,2048]{1,0:T(2,128)} %param.28) | copy-start | bytes 49156
  347.8 21.6 %copy-start.1 = (bf16[256,512]{1,0:T(8,128)(2,1)S(1)}, bf16[256,512]{1,0:T(8,128)(2,1)}, u32[]{:S(2)}) copy-start(bf16[256,512]{1,0:T(8,128)(2,1)} %param.26) | copy-start | bytes 786436
  349.4 19.9 %all-to-all-start.2 = ((bf16[4,256,512]{2,1,0:T(8,128)(2,1)}), bf16[4,256,512]{2,1,0:T(8,128)(2,1)S(1)}, u32[]{:S(2)}, u32[]{:S(2)}) async-start(bf16[4,256,512]{2,1,0:T(8,128)(2,1)} %bitcast.317), calls=%async_computation.2 | async-start | bytes 2097152 | tf_op jit(solution)/shard_map/all_to_all | solution.py:87
  370.2 8.6 %all-to-all-start.3 = ((f32[4,1,512]{2,1,0:T(1,128)}), f32[4,1,512]{2,1,0:T(1,128)S(1)}, u32[]{:S(2)}, u32[]{:S(2)}) async-start(f32[4,1,512]{2,1,0:T(1,128)} %broadcast_in_dim.211), calls=%async_computation.3 | async-start | bytes 16384 | tf_op jit(solution)/shard_map/all_to_all | solution.py:17
  422.0 8.6 %all-to-all-start.6 = ((f32[4,1,512]{2,1,0:T(1,128)}), f32[4,1,512]{2,1,0:T(1,128)S(1)}, u32[]{:S(2)}, u32[]{:S(2)}) async-start(f32[4,1,512]{2,1,0:T(1,128)} %broadcast_in_dim.213), calls=%async_computation.6 | async-start | bytes 16384 | tf_op jit(solution)/shard_map/all_to_all | solution.py:17
Sparse Core Ops, SparseCore 0:
  126.9 104.1 all-gather.1
where the time goes:
time: 442 us; the launch traced here: 438 us
  local copies, waits for them, and re-layouts  141 us (32%)
  other arithmetic  92.2 us (21%)
  waiting for transfers between devices  69.8 us (16%)
  starting transfers between devices  49 us (11%)
  blocking collectives  30.2 us (7%)
  between operations  26.3 us (6%)
  matrix products  19.9 us (5%)
  loops' own time  9.81 us (2%)
    all_to_all x4, waiting for transfers between devices, sent_to_all(): lax.all_to_all(jnp.broadcast_to(x[None], (peers, *x.shape)), axis, 0, 0,...  54.5 us
    while x8, local copies, waits for them, and re-layouts  46.9 us
    all_to_all x4, starting transfers between devices, sent_to_all(): lax.all_to_all(jnp.broadcast_to(x[None], (peers, *x.shape)), axis, 0, 0,...  44.1 us
    dynamic_update_slice x8, local copies, waits for them, and re-layouts, run_blocks(): lax.scan(advance, start, tuple((blocked(array) for array in (query, key_p...  29.1 us
    while x8, other arithmetic  25.6 us
    dot_general x8, other arithmetic, advance(): jnp.einsum('ihd,jhd,ijhd->hij', query_block, key_block, relative, precisi...  23.1 us
    all_to_all x1, blocking collectives, sent_to_all(): lax.all_to_all(jnp.broadcast_to(x[None], (peers, *x.shape)), axis, 0, 0,...  15.7 us
    all_to_all x1, waiting for transfers between devices, summed_on_arrival(): parts = lax.all_to_all(cut_along(x, dim, peers), axis, 0, 0, tiled=True)  15.2 us
  transfers between devices with their start and end apart: 6, of which 4 were waited for; matrix products, arithmetic and copies ran while one was open for 35% of the time, Pallas kernels for 0%

commit v1 on v0

v1 whole, which is shorter than its diff:
```python
import functools
import jax
import jax.numpy as jnp
from jax import lax
from jax.experimental import pallas as pl
from jax.experimental.pallas import tpu as pltpu
from jax.sharding import PartitionSpec as P

DK = 32
DV = 64
DOCS = 4
EPS = 1e-06
META = 8
F32 = jnp.float32
BF = jnp.bfloat16


def iota(shape, dim):
    return lax.broadcasted_iota(jnp.int32, shape, dim)

def mm(a, b, dims=((1,), (0,))):
    return lax.dot_general(a, b, (dims, ((), ())), preferred_element_type=F32)

def partner(total, upper, h):
    n = total.shape[0]
    return jnp.where(upper, pltpu.roll(total, h, 0), pltpu.roll(total, n - h, 0))

def levels(g, r):
    n = g.shape[0]
    row = iota(g.shape, 0)
    zero = jnp.zeros_like(g)
    gi, gx, ri, rx, gt, rt = g, zero, r, zero, g, r
    h = 1
    while h < n:
        upper = (row & h) != 0
        yield h, jnp.where(upper, gi, ri), jnp.where(upper, rx, gx)
        gp, rp = partner(gt, upper, h), partner(rt, upper, h)
        gi = jnp.where(upper, gi + gp, gi)
        gx = jnp.where(upper, gx, gx + gp)
        ri = jnp.where(upper, ri, ri + rp)
        rx = jnp.where(upper, rx + rp, rx)
        gt, rt = gt + gp, rt + rp
        h *= 2
    yield n, (gi, gx, gt), (ri, rx, rt)

def rows_of(docs_row):
    n = docs_row.shape[1]
    return jnp.broadcast_to(docs_row, (128, n)).T

def head_block(kw, vw):
    return (iota((kw, vw), 0) // DK) == (iota((kw, vw), 1) // DV)

def state_of(keys, values):
    kw, vw = keys.shape[1], values.shape[1]
    full = mm(keys.astype(BF), values, ((0,), (0,)))
    full = jnp.where(head_block(kw, vw), full, 0.0)
    return functools.reduce(jnp.add, [full[a : a + DK] for a in range(0, kw, DK)])

def packed(state, passing, entry, leaving):
    vw = state.shape[1]
    wide = jnp.concatenate([passing] * (vw // passing.shape[1]), axis=1)
    line = iota((META, vw), 0)
    entry = jnp.concatenate([entry] * (vw // entry.shape[1]), axis=1)
    leaving = jnp.concatenate([leaving] * (vw // leaving.shape[1]), axis=1)
    meta = jnp.where(line == 0, wide, jnp.where(line == 1, entry, leaving))
    return jnp.concatenate([state, meta], axis=0).astype(BF)

def states_kernel(q_ref, k_ref, v_ref, d_ref, doc_ref, qf_ref, qb_ref, f_ref, b_ref):
    n, kw = q_ref.shape
    docs = rows_of(doc_ref[...].astype(F32))
    first, last = docs[0:1], docs[n - 1 : n]
    for h, fwd, bwd in levels(d_ref[0], d_ref[1]):
        if h == n:
            break
    gi, gx, gt = fwd
    ri, rx, rt = bwd
    q = q_ref[...].astype(F32) * DK ** (-0.5)
    k = k_ref[...].astype(F32)
    v = v_ref[...]
    qf_ref[...] = (q * jnp.exp(gi)).astype(BF)
    qb_ref[...] = (q * jnp.exp(ri)).astype(BF)
    through = jnp.where(first == last, 1.0, 0.0)
    f_ref[...] = packed(
        state_of(jnp.where(docs == last, k * jnp.exp(gx), 0.0), v),
        jnp.exp(gt[0:1]) * through, first, last)
    b_ref[...] = packed(
        state_of(jnp.where(docs == first, k * jnp.exp(rx), 0.0), v),
        jnp.exp(rt[0:1]) * through, last, first)

def spread(passing, vw):
    kw = passing.shape[1]
    place = (iota((DK, kw), 1) % DK) == iota((DK, kw), 0)
    picked = jnp.where(place, jnp.broadcast_to(passing, (DK, kw)), 0.0)
    return mm(picked.astype(BF), jnp.where(head_block(kw, vw), 1.0, 0.0).astype(BF))

def chain3(near, mid, far, kw):
    vw = near.shape[1]
    n, m, f = near.astype(F32), mid.astype(F32), far.astype(F32)
    top = lambda a: a[:DK]
    line = lambda a, j: a[DK + j : DK + j + 1]
    keep1 = jnp.where(line(n, 1) == line(m, 2), 1.0, 0.0)
    keep2 = jnp.where(line(m, 1) == line(f, 2), 1.0, 0.0)
    p1 = (line(n, 0) * keep1)[:, :kw]
    p2 = (line(m, 0) * keep2)[:, :kw]
    state = top(n) + spread(p1, vw) * (top(m) + spread(p2, vw) * top(f))
    return state, p1 * p2 * line(f, 0)[:, :kw], line(f, 1), line(n, 2)

def fold_kernel(f1, f2, f3, b1, b2, b3, f_ref, b_ref, *, kw):
    for refs, out in (((f1, f2, f3), f_ref), ((b1, b2, b3), b_ref)):
        state, passing, entry, leaving = chain3(*(x[...] for x in refs), kw)
        out[...] = packed(state, passing, entry[:, :kw], leaving[:, :kw])

def local_kernel(q_ref, k_ref, v_ref, d_ref, doc_ref, out_ref, qe_ref, ke_ref):
    n, kw = q_ref.shape
    vw = v_ref.shape[1]
    half = n // 2
    heads = kw // DK
    q = q_ref[...].astype(F32) * DK ** (-0.5)
    k = k_ref[...].astype(F32)
    hs = []
    for h, eq, ek in levels(d_ref[0], d_ref[1]):
        if h < n:
            qe_ref[len(hs)] = (q * jnp.exp(eq)).astype(BF)
            ke_ref[len(hs)] = (k * jnp.exp(ek)).astype(BF)
            hs.append(h)
    drow = doc_ref[...].astype(F32)
    dcol = rows_of(drow)
    v = v_ref[...]
    lane = iota((half, kw), 1) // DK
    olane = iota((half, vw), 1) // DV
    apart = iota((half, half), 0) ^ iota((half, half), 1)
    ones = jnp.where(head_block(kw, vw), 2.0, 0.0).astype(BF)
    same = mm((q * k).astype(BF), ones) * v.astype(F32)
    for t in range(2):
        mine = slice(t * half, (t + 1) * half)
        other = slice((1 - t) * half, (2 - t) * half)
        ok_in = (dcol[mine] == drow[:, mine]) & (apart != 0)
        ok_off = dcol[mine] == drow[:, other]
        acc = same[mine]
        for head in range(heads):
            own = lane == head
            score = None
            for l, h in enumerate(hs[:-1]):
                prod = mm(jnp.where(own, qe_ref[l, mine], 0), ke_ref[l, mine], ((1,), (1,)))
                score = prod if score is None else jnp.where(apart >= h, prod, score)
            off = mm(jnp.where(own, qe_ref[len(hs) - 1, mine], 0), ke_ref[len(hs) - 1, other], ((1,), (1,)))
            score = jnp.where(ok_in, score, 0.0).astype(BF)
            off = jnp.where(ok_off, off, 0.0).astype(BF)
            res = mm(score, v[mine]) + mm(off, v[other])
            acc = acc + jnp.where(olane == head, res, 0.0)
        out_ref[mine] = acc

def mix_kernel(local_ref, qf_ref, qb_ref, doc_ref, gate_ref, gain_ref, f1, f2, f3, b1, b2, b3, out_ref):
    n, kw = qf_ref.shape
    vw = local_ref.shape[1]
    docs = rows_of(doc_ref[...].astype(F32))
    out = local_ref[...]
    block = head_block(kw, vw)
    for q_ref, refs in ((qf_ref, (f1, f2, f3)), (qb_ref, (b1, b2, b3))):
        state, _, _, leaving = chain3(*(x[...] for x in refs), kw)
        wide = jnp.where(block, jnp.concatenate([state] * (kw // DK), axis=0), 0.0)
        reach = jnp.where(docs[:, :kw] == leaving[:, :kw], q_ref[...], 0)
        out = out + mm(reach, wide.astype(BF))
    square = out * out
    high = square.astype(BF)
    low = (square - high.astype(F32)).astype(BF)
    mean = jnp.where((iota((vw, vw), 0) // DV) == (iota((vw, vw), 1) // DV), 1.0 / DV, 0.0).astype(BF)
    power = mm(high, mean) + mm(low, mean)
    gate = gate_ref[...].astype(F32)
    out_ref[...] = (out * lax.rsqrt(power + EPS) * gain_ref[...] * (gate / (1.0 + jnp.exp(-gate)))).astype(BF)

def call(kernel, outs, args, scratch=(), flops=1 << 26):
    return pl.pallas_call(
        kernel, out_shape=outs, scratch_shapes=scratch,
        in_specs=[pl.BlockSpec(memory_space=pltpu.VMEM)] * len(args),
        out_specs=jax.tree.map(lambda _: pl.BlockSpec(memory_space=pltpu.VMEM), outs),
        cost_estimate=pl.CostEstimate(flops=flops, bytes_accessed=1 << 20, transcendentals=1 << 17),
    )(*args)

SDS = jax.ShapeDtypeStruct
def states(q,k,v,d,doc):
    n,kw=q.shape; vw=v.shape[1]
    return call(states_kernel,(SDS((n,kw),BF),)*2+(SDS((DK+META,vw),BF),)*2,(q,k,v,d,doc))
def fold(parts,kw):
    vw=parts[0].shape[1]
    return call(functools.partial(fold_kernel,kw=kw),(SDS((DK+META,vw),BF),)*2,parts)
def local(q,k,v,d,doc):
    n,kw=q.shape; vw=v.shape[1]; L=n.bit_length()-1
    return call(local_kernel,SDS((n,vw),F32),(q,k,v,d,doc),(pltpu.VMEM((L,n,kw),BF),)*2,flops=1<<29)
def mix(local,qf,qb,doc,gate,gain,parts):
    return call(mix_kernel,SDS(local.shape,BF),(local,qf,qb,doc,gate,gain,*parts))


def ring(axis, step):
    peers = lax.axis_size(axis)
    return [(i, (i + step) % peers) for i in range(peers)]


def line(axis, step):
    peers = lax.axis_size(axis)
    return [(i, i + step) for i in range(peers) if 0 <= i + step < peers]


def carried(f, b, kw, reach):
    step = 1
    while True:
        shifts = (1, 2, 3) if step == 1 else (step, 2 * step)
        near = [lax.ppermute(f, "sp", line("sp", s)) for s in shifts]
        far = [lax.ppermute(b, "sp", line("sp", -s)) for s in shifts]
        if step > 1:
            near, far = [f] + near, [b] + far
        step *= 3
        if step >= reach:
            return tuple(near + far)
        f, b = fold(tuple(near + far), kw)


def from_peers(parts, axis):
    return [lax.ppermute(parts[s], axis, ring(axis, s)) for s in range(1, len(parts))]


def part_of(x, number, peers):
    width = x.shape[1] // peers
    return lax.dynamic_slice_in_dim(x, number * width, width, 1)


def summed(mine, axis):
    return mine + sum(from_peers([mine] * lax.axis_size(axis), axis))


def normed(stream, full_width, gain, bias):
    total = summed(jnp.stack([jnp.sum(stream, axis=1), jnp.sum(stream * stream, axis=1)]), "tp")
    middle = total[0][:, None] / full_width
    spread_ = total[1][:, None] / full_width - middle * middle
    return (stream - middle) * lax.rsqrt(spread_ + EPS) * gain + bias


def inner_kernel(at_ref, x0, x1, x2, x3, gate_ref, up_ref, out_ref):
    gate, up = None, None
    for s, x in enumerate((x0, x1, x2, x3)):
        depth = x.shape[1]
        rows = pl.ds(pl.multiple_of(at_ref[s] * depth, depth), depth)
        g, u = mm(x[...], gate_ref[rows, :]), mm(x[...], up_ref[rows, :])
        gate, up = (g, u) if s == 0 else (gate + g, up + u)
    out_ref[...] = (gate / (1.0 + jnp.exp(-gate)) * up).astype(BF)


def inner_of(at, pieces, weights, hidden):
    n, depth = pieces[0].shape
    full = weights.shape[0]
    block = 256
    steps = hidden // block
    return pl.pallas_call(
        inner_kernel,
        out_shape=SDS((n, hidden), BF),
        grid_spec=pltpu.PrefetchScalarGridSpec(
            num_scalar_prefetch=1,
            grid=(steps,),
            in_specs=[pl.BlockSpec((n, depth), lambda i, at: (0, 0))] * 4
            + [pl.BlockSpec((full, block), lambda i, at: (0, i)),
               pl.BlockSpec((full, block), lambda i, at: (0, i + steps))],
            out_specs=pl.BlockSpec((n, block), lambda i, at: (0, i)),
        ),
        cost_estimate=pl.CostEstimate(flops=4 * n * full * hidden, bytes_accessed=4 * full * hidden, transcendentals=n * hidden),
    )(at, *pieces, weights, weights)


def down_kernel(at_ref, x_ref, w_ref, out_ref):
    out_ref[...] = mm(x_ref[...], w_ref[...], ((1,), (1,))).astype(BF)


def down_of(at, inner, weights, width):
    n, hidden = inner.shape
    return pl.pallas_call(
        down_kernel,
        out_shape=SDS((n, width), BF),
        grid_spec=pltpu.PrefetchScalarGridSpec(
            num_scalar_prefetch=1,
            grid=(1,),
            in_specs=[pl.BlockSpec((n, hidden), lambda i, at: (0, 0)),
                      pl.BlockSpec((width, hidden), lambda i, at: (at[0], 2))],
            out_specs=pl.BlockSpec((n, width), lambda i, at: (0, 0)),
        ),
        cost_estimate=pl.CostEstimate(flops=2 * n * hidden * width, bytes_accessed=2 * hidden * width, transcendentals=0),
    )(at, inner, weights)


def on_device(
    queries, key_rows, value_rows, out_gate, log_decay, doc_ids, head_gain, out_weight,
    residual, norm_gain, norm_bias, gate_weight, up_weight, down_weight,
):
    peers, me = lax.axis_size("tp"), lax.axis_index("tp")
    length, kw = queries.shape
    hidden = gate_weight.shape[1]
    weights = lax.all_gather(
        jnp.concatenate([gate_weight, up_weight, down_weight.T], axis=1), "sp", axis=0, tiled=True
    )
    docs = doc_ids[None]
    qf, qb, f, b = states(queries, key_rows, value_rows, log_decay, docs)
    reach = -(-length * lax.axis_size("sp") // DOCS // length) + 1
    parts = carried(f, b, kw, reach)
    near = local(queries, key_rows, value_rows, log_decay, docs)
    mixed = mix(near, qf, qb, docs, out_gate, head_gain[None], parts)
    partial = jnp.dot(mixed, out_weight, preferred_element_type=F32).astype(BF)
    mine = [part_of(partial, (me + s) % peers, peers) for s in range(peers)]
    branch = sum(x.astype(F32) for x in [mine[0]] + from_peers(mine, "tp"))
    own_width = residual.shape[1]
    full_width = own_width * peers
    own = lambda table, j: lax.dynamic_slice_in_dim(table[j], me * own_width, own_width, 0)
    settled = normed(residual.astype(F32) + branch, full_width, own(norm_gain, 0), own(norm_bias, 0))
    features = settled.astype(BF)
    pieces = [features] + from_peers([features] * peers, "tp")
    at = jnp.stack([(me - s) % peers for s in range(peers)]).astype(jnp.int32)
    inner = inner_of(at, pieces, weights, hidden)
    down = [None] * peers
    for s in [2, 1, 3, 0]:
        down[s] = down_of(((me + s) % peers).astype(jnp.int32)[None], inner, weights, own_width)
    total = sum(x.astype(F32) for x in [down[0]] + from_peers(down, "tp"))
    result = normed(settled + 0.5 * total, full_width, own(norm_gain, 1), own(norm_bias, 1))
    return result.astype(BF)


def solution(mesh):
    rows = ("grp", "sp")
    in_specs = (
        P(rows, "tp"), P(rows, "tp"), P(rows, "tp"), P(rows, "tp"), P(None, rows, "tp"),
        P(rows), P("tp"), P("tp", None), P(rows, "tp"), P(), P(),
        P("sp", "tp"), P("sp", "tp"), P("tp", "sp"),
    )
    return jax.shard_map(
        on_device, mesh=mesh, in_specs=in_specs, out_specs=P(rows, "tp"), check_vma=False
    )
```

time: 442 us -> 157 us (0.36)
  local copies, waits for them, and re-layouts: 141 us -> 3.65 us
  other arithmetic: 92.2 us -> 6.11 us
  blocking collectives: 30.2 us -> 0 us
  waiting for transfers between devices: 69.8 us -> 41.7 us
  Pallas kernels: 0 us -> 27 us
  matrix products: 19.9 us -> 1.35 us
  starting transfers between devices: 49 us -> 61.7 us
  between operations: 26.3 us -> 13.7 us
  loops' own time: 9.81 us -> 0 us
    all_to_all x5 -> x0, waiting for transfers between devices: 69.7 us -> none  [the longest x4 54.5 us: sent_to_all(): lax.all_to_all(jnp.broadcast_to(x[None], (peers, *x.shape)), axis, 0, 0,...]
    ppermute x0 -> x25, starting transfers between devices: none -> 61.7 us  [the longest x5 30.3 us: carried(): near = [lax.ppermute(f, 'sp', line('sp', s)) for s in shifts]]
    all_to_all x5 -> x0, starting transfers between devices: 48.7 us -> none  [the longest x4 44.1 us: sent_to_all(): lax.all_to_all(jnp.broadcast_to(x[None], (peers, *x.shape)), axis, 0, 0,...]
    while x8 -> x0, local copies, waits for them, and re-layouts: 46.9 us -> none
    ppermute x0 -> x25, waiting for transfers between devices: none -> 41.6 us  [the longest x15 30.2 us: from_peers(): lax.ppermute(parts[s], axis, ring(axis, s))]
    all_to_all x2 -> x0, blocking collectives: 30.2 us -> none  [the longest x1 15.7 us: sent_to_all(): lax.all_to_all(jnp.broadcast_to(x[None], (peers, *x.shape)), axis, 0, 0,...]
    dynamic_update_slice x8 -> x0, local copies, waits for them, and re-layouts: 29.1 us -> none  [run_blocks(): lax.scan(advance, start, tuple((blocked(array) for array in (query, key_p...]
    pallas_call x0 -> x9, Pallas kernels: none -> 27 us  [the longest x4 11.1 us: call(): pl.pallas_call(kernel, out_shape=outs, scratch_shapes=scratch, in_specs=[...]
  transfers between devices with their start and end apart: 6 -> 26, of which waited for: 4 -> 14; matrix products, arithmetic and copies ran while one was open for 35% -> 3% of each run, Pallas kernels for 0% -> 12%
where the time goes in v1:
time: 157 us; the launch traced here: 155 us
  starting transfers between devices  61.7 us (39%)
  waiting for transfers between devices  41.7 us (27%)
  Pallas kernels  27 us (17%)
  between operations  13.7 us (9%)
  other arithmetic  6.11 us (4%)
  local copies, waits for them, and re-layouts  3.65 us (2%)
    ppermute x5, starting transfers between devices, carried(): near = [lax.ppermute(f, 'sp', line('sp', s)) for s in shifts]  30.3 us
    ppermute x15, waiting for transfers between devices, from_peers(): lax.ppermute(parts[s], axis, ring(axis, s))  30.2 us
    ppermute x15, starting transfers between devices, from_peers(): lax.ppermute(parts[s], axis, ring(axis, s))  24.9 us
    ppermute x5, waiting for transfers between devices, carried(): far = [lax.ppermute(b, 'sp', line('sp', -s)) for s in shifts]  11.4 us
    pallas_call x4, Pallas kernels, call(): pl.pallas_call(kernel, out_shape=outs, scratch_shapes=scratch, in_specs=[...  11.1 us
    pallas_call x4, Pallas kernels, down_of(): pl.pallas_call(down_kernel, out_shape=SDS((n, width), BF), grid_spec=pltp...  9.48 us
    ppermute x5, starting transfers between devices, carried(): far = [lax.ppermute(b, 'sp', line('sp', -s)) for s in shifts]  6.54 us
    pallas_call x1, Pallas kernels, inner_of(): pl.pallas_call(inner_kernel, out_shape=SDS((n, hidden), BF), grid_spec=pl...  6.33 us
  transfers between devices with their start and end apart: 26, of which 14 were waited for; matrix products, arithmetic and copies ran while one was open for 3% of the time, Pallas kernels for 12%

profile of v1, /device:TPU:40, one launch (start us, length us, event | category | flops | bytes accessed | tf_op | source)
XLA Modules:
  0.0 155.1 jit_solution(9401083518013944993)
XLA Ops:
  6.6 1.8 %pad_maximum_fusion = bf16[64,2304]{1,0:T(8,128)(2,1)} fusion(bf16[64,768]{1,0:T(8,128)(2,1)} %bitcast.24, bf16[64,768]{1,0:T(8,128)(2,1)} %param.26, bf16[64,768]{1,0:T(8,128)(2,1)} %param.25), kind=kLoop, calls=%fused_computation.8 | loop fusion | flops 884736 | bytes 589824 | tf_op jit(solution)/shard_map/concatenate | solution.py:296
  8.4 2.3 %shard_map.137 = (bf16[256,128]{1,0:T(8,128)(2,1)}, bf16[256,128]{1,0:T(8,128)(2,1)}, bf16[40,256]{1,0:T(8,128)(2,1)}, bf16[40,256]{1,0:T(8,128)(2,1)}) custom-call(bf16[256,128]{1,0:T(8,128)(2,1)} %q_ref.3, bf16[256,128]{1,0:T(8,128)(2,1)} %k_ref.3, bf16[256,256]{1,0:T(8,128)(2,1)} %v_ref.3, f32[2,256,128]{2,1,0:T(8,128)} %d_ref.3, s32[1,256]{1,0:T(1,128)} %bitcast.44), custom_call_target="tpu_custom_call" | custom-call | flops 67108864 | bytes 1048576 | tf_op jit(solution)/shard_map/pallas_call | solution.py:173
  10.8 1.8 %collective-permute-start = (bf16[40,256]{1,0:T(8,128)(2,1)}, bf16[40,256]{1,0:T(8,128)(2,1)S(1)}, u32[]{:S(2)}, u32[]{:S(2)}) collective-permute-start(bf16[40,256]{1,0:T(8,128)(2,1)} %get-tuple-element.13), channel_id=1, source_target_pairs={{0,4},{4,8},{8,12},{12,16},{16,20},{20,24},{24,28},{28,32},{32,36}... | collective-permute-start | bytes 61448 | tf_op jit(solution)/shard_map/ppermute | solution.py:208
  12.6 4.8 %collective-permute-start.1 = (bf16[40,256]{1,0:T(8,128)(2,1)}, bf16[40,256]{1,0:T(8,128)(2,1)S(1)}, u32[]{:S(2)}, u32[]{:S(2)}) collective-permute-start(bf16[40,256]{1,0:T(8,128)(2,1)} %get-tuple-element.13), channel_id=1, source_target_pairs={{0,8},{4,12},{8,16},{12,20},{16,24},{20,28},{24,32},{28,36},{32,40... | collective-permute-start | bytes 61448 | tf_op jit(solution)/shard_map/ppermute | solution.py:208
  17.4 6.9 %collective-permute-start.2 = (bf16[40,256]{1,0:T(8,128)(2,1)}, bf16[40,256]{1,0:T(8,128)(2,1)S(1)}, u32[]{:S(2)}, u32[]{:S(2)}) collective-permute-start(bf16[40,256]{1,0:T(8,128)(2,1)} %get-tuple-element.13), channel_id=1, source_target_pairs={{0,12},{4,16},{8,20},{12,24},{16,28},{20,32},{24,36},{28,40},{32,4... | collective-permute-start | bytes 61448 | tf_op jit(solution)/shard_map/ppermute | solution.py:208
  24.4 1.3 collective-permute-start.3
  25.7 1.3 collective-permute-start.4
  27.0 1.3 collective-permute-start.5
  28.3 0.8 fusion.3
  29.2 5.0 %collective-permute-done.4.b2 = bf16[40,256]{1,0:T(8,128)(2,1)S(1)} collective-permute-done((bf16[40,256]{1,0:T(8,128)(2,1)}, bf16[40,256]{1,0:T(8,128)(2,1)S(1)}, u32[]{:S(2)}, u32[]{:S(2)}) %collective-permute-start.4) | collective-permute-done | bytes 20512 | tf_op jit(solution)/shard_map/ppermute | solution.py:209
  34.2 1.8 %collective-permute-done.5.b3 = bf16[40,256]{1,0:T(8,128)(2,1)S(1)} collective-permute-done((bf16[40,256]{1,0:T(8,128)(2,1)}, bf16[40,256]{1,0:T(8,128)(2,1)S(1)}, u32[]{:S(2)}, u32[]{:S(2)}) %collective-permute-start.5) | collective-permute-done | bytes 20512 | tf_op jit(solution)/shard_map/ppermute | solution.py:209
  36.6 1.6 %shard_map.138 = (bf16[40,256]{1,0:T(8,128)(2,1)}, bf16[40,256]{1,0:T(8,128)(2,1)}) custom-call(bf16[40,256]{1,0:T(8,128)(2,1)} %copy-done.9, bf16[40,256]{1,0:T(8,128)(2,1)} %copy-done.10, bf16[40,256]{1,0:T(8,128)(2,1)} %copy-done.11, bf16[40,256]{1,0:T(8,128)(2,1)} %copy-done.12, bf16[40,256]{1,0:T(8,128)(2,1)} %copy-done.13, bf16[40,256]{1,0:T(8,128)(2,1)} %copy-done.14), custom_call_target="tpu_custom_call" | custom-call | flops 67108864 | bytes 1048576 | tf_op jit(solution)/shard_map/pallas_call | solution.py:173
  38.3 6.6 %collective-permute-start.6 = (bf16[40,256]{1,0:T(8,128)(2,1)}, bf16[40,256]{1,0:T(8,128)(2,1)S(1)}, u32[]{:S(2)}, u32[]{:S(2)}) collective-permute-start(bf16[40,256]{1,0:T(8,128)(2,1)} %get-tuple-element.15.f1), channel_id=1, source_target_pairs={{0,12},{4,16},{8,20},{12,24},{16,28},{20,32},{24,36},{28,40},{32,4... | collective-permute-start | bytes 61448 | tf_op jit(solution)/shard_map/ppermute | solution.py:208
  44.9 10.1 %collective-permute-start.7 = (bf16[40,256]{1,0:T(8,128)(2,1)}, bf16[40,256]{1,0:T(8,128)(2,1)S(1)}, u32[]{:S(2)}, u32[]{:S(2)}) collective-permute-start(bf16[40,256]{1,0:T(8,128)(2,1)} %get-tuple-element.15.f1), channel_id=1, source_target_pairs={{0,24},{4,28},{8,32},{12,36},{16,40},{20,44},{24,48},{28,52},{32,5... | collective-permute-start | bytes 61448 | tf_op jit(solution)/shard_map/ppermute | solution.py:208
  55.0 1.3 collective-permute-start.8
  56.3 1.3 collective-permute-start.9
  57.6 4.7 %shard_map.136.local_ref = f32[256,256]{1,0:T(8,128)} custom-call(bf16[256,128]{1,0:T(8,128)(2,1)} %q_ref.3, bf16[256,128]{1,0:T(8,128)(2,1)} %k_ref.3, bf16[256,256]{1,0:T(8,128)(2,1)} %v_ref.3, f32[2,256,128]{2,1,0:T(8,128)} %d_ref.3, s32[1,256]{1,0:T(1,128)} %bitcast.45), custom_call_target="tpu_custom_call" | custom-call | flops 536870912 | bytes 1048576 | tf_op jit(solution)/shard_map/pallas_call | solution.py:173
  62.4 4.6 %collective-permute-done.9.b3 = bf16[40,256]{1,0:T(8,128)(2,1)S(1)} collective-permute-done((bf16[40,256]{1,0:T(8,128)(2,1)}, bf16[40,256]{1,0:T(8,128)(2,1)S(1)}, u32[]{:S(2)}, u32[]{:S(2)}) %collective-permute-start.9) | collective-permute-done | bytes 20512 | tf_op jit(solution)/shard_map/ppermute | solution.py:209
  67.6 2.4 %shard_map.139 = bf16[256,256]{1,0:T(8,128)(2,1)} custom-call(f32[256,256]{1,0:T(8,128)} %shard_map.136.local_ref, bf16[256,128]{1,0:T(8,128)(2,1)} %get-tuple-element.11.qf_ref, bf16[256,128]{1,0:T(8,128)(2,1)} %get-tuple-element.12.qb_ref, s32[1,256]{1,0:T(1,128)} %bitcast.46, bf16[256,256]{1,0:T(8,128)(2,1)} %gate_ref.1, f32[1,256]{1,0:T(1,128)} %bitcast.49, ...), custom_call_target="tpu_custom_call" | custom-call | flops 67108864 | bytes 1048576 | tf_op jit(solution)/shard_map/pallas_call | solution.py:173
  70.1 1.3 convolution_convert_fusion
  71.5 1.9 %collective-permute-start.10 = (bf16[256,512]{1,0:T(8,128)(2,1)S(1)}, bf16[256,512]{1,0:T(8,128)(2,1)S(1)}, u32[]{:S(2)}, u32[]{:S(2)}) collective-permute-start(bf16[256,512]{1,0:T(8,128)(2,1)S(1)} %get-tuple-element.23), channel_id=1, source_target_pairs={{0,1},{1,2},{2,3},{3,0},{4,5},{5,6},{6,7},{7,4},{8,9},{9,10},{10,1... | collective-permute-start | bytes 786440 | tf_op jit(solution)/shard_map/ppermute | solution.py:219
  73.4 2.6 %collective-permute-start.11 = (bf16[256,512]{1,0:T(8,128)(2,1)S(1)}, bf16[256,512]{1,0:T(8,128)(2,1)S(1)}, u32[]{:S(2)}, u32[]{:S(2)}) collective-permute-start(bf16[256,512]{1,0:T(8,128)(2,1)S(1)} %get-tuple-element.25), channel_id=1, source_target_pairs={{0,2},{1,3},{2,0},{3,1},{4,6},{5,7},{6,4},{7,5},{8,10},{9,11},{10,... | collective-permute-start | bytes 786440 | tf_op jit(solution)/shard_map/ppermute | solution.py:219
  75.9 1.7 %collective-permute-start.12 = (bf16[256,512]{1,0:T(8,128)(2,1)S(1)}, bf16[256,512]{1,0:T(8,128)(2,1)S(1)}, u32[]{:S(2)}, u32[]{:S(2)}) collective-permute-start(bf16[256,512]{1,0:T(8,128)(2,1)S(1)} %get-tuple-element.24), channel_id=1, source_target_pairs={{0,3},{1,0},{2,1},{3,2},{4,7},{5,4},{6,5},{7,6},{8,11},{9,8},{10,9... | collective-permute-start | bytes 786440 | tf_op jit(solution)/shard_map/ppermute | solution.py:219
  78.4 2.7 %collective-permute-done.10 = bf16[256,512]{1,0:T(8,128)(2,1)S(1)} collective-permute-done((bf16[256,512]{1,0:T(8,128)(2,1)S(1)}, bf16[256,512]{1,0:T(8,128)(2,1)S(1)}, u32[]{:S(2)}, u32[]{:S(2)}) %collective-permute-start.10) | collective-permute-done | bytes 262176 | tf_op jit(solution)/shard_map/ppermute | solution.py:219
  81.1 6.3 %collective-permute-done.11 = bf16[256,512]{1,0:T(8,128)(2,1)S(1)} collective-permute-done((bf16[256,512]{1,0:T(8,128)(2,1)S(1)}, bf16[256,512]{1,0:T(8,128)(2,1)S(1)}, u32[]{:S(2)}, u32[]{:S(2)}) %collective-permute-start.11) | collective-permute-done | bytes 262176 | tf_op jit(solution)/shard_map/ppermute | solution.py:219
  87.4 1.2 fusion.2
  88.7 1.5 collective-permute-start.13
  90.2 2.4 %collective-permute-start.14 = (f32[2,256]{1,0:T(2,128)S(1)}, f32[2,256]{1,0:T(2,128)S(1)}, u32[]{:S(2)}, u32[]{:S(2)}) collective-permute-start(f32[2,256]{1,0:T(2,128)S(1)} %pad_maximum_fusion.1), channel_id=1, source_target_pairs={{0,2},{1,3},{2,0},{3,1},{4,6},{5,7},{6,4},{7,5},{8,10},{9,11},{10,... | collective-permute-start | bytes 6152 | tf_op jit(solution)/shard_map/ppermute | solution.py:219
  92.6 1.9 %collective-permute-start.15 = (f32[2,256]{1,0:T(2,128)S(1)}, f32[2,256]{1,0:T(2,128)S(1)}, u32[]{:S(2)}, u32[]{:S(2)}) collective-permute-start(f32[2,256]{1,0:T(2,128)S(1)} %pad_maximum_fusion.1), channel_id=1, source_target_pairs={{0,3},{1,0},{2,1},{3,2},{4,7},{5,4},{6,5},{7,6},{8,11},{9,8},{10,9... | collective-permute-start | bytes 6152 | tf_op jit(solution)/shard_map/ppermute | solution.py:219
  94.4 0.8 collective-permute-done.14
  95.2 0.9 collective-permute-done.15
  97.2 3.8 %collective-permute-start.17 = (bf16[256,512]{1,0:T(8,128)(2,1)S(1)}, bf16[256,512]{1,0:T(8,128)(2,1)S(1)}, u32[]{:S(2)}, u32[]{:S(2)}) collective-permute-start(bf16[256,512]{1,0:T(8,128)(2,1)S(1)} %fusion.x0), channel_id=1, source_target_pairs={{0,2},{1,3},{2,0},{3,1},{4,6},{5,7},{6,4},{7,5},{8,10},{9,11},{10,... | collective-permute-start | bytes 786440 | tf_op jit(solution)/shard_map/ppermute | solution.py:219
  101.6 8.7 %collective-permute-done.16.x1 = bf16[256,512]{1,0:T(8,128)(2,1)S(1)} collective-permute-done((bf16[256,512]{1,0:T(8,128)(2,1)S(1)}, bf16[256,512]{1,0:T(8,128)(2,1)S(1)}, u32[]{:S(2)}, u32[]{:S(2)}) %collective-permute-start.16) | collective-permute-done | bytes 262176 | tf_op jit(solution)/shard_map/ppermute | solution.py:219
  111.6 6.3 %shard_map.140.x_ref = bf16[256,768]{1,0:T(8,128)(2,1)} custom-call(s32[4]{0:T(128)} %pad_add_fusion.at_ref, bf16[256,512]{1,0:T(8,128)(2,1)} %copy-done.1, bf16[256,512]{1,0:T(8,128)(2,1)} %copy-done.2, bf16[256,512]{1,0:T(8,128)(2,1)} %copy-done.3, bf16[256,512]{1,0:T(8,128)(2,1)} %copy-done.4, ...), custom_call_target="tpu_custom_call" | custom-call | flops 1610612736 | bytes 6291456 | tf_op jit(solution)/shard_map/pallas_call | solution.py:253
  118.0 2.4 %shard_map.142 = bf16[256,512]{1,0:T(8,128)(2,1)} custom-call(s32[1]{0:T(128)} %bitcast.13.at_ref, bf16[256,768]{1,0:T(8,128)(2,1)} %shard_map.140.x_ref, bf16[2048,2304]{1,0:T(8,128)(2,1)} %all-gather.2.cloned.1.call-done.gate_ref.up_ref.w_ref), custom_call_target="tpu_custom_call" | custom-call | flops 201326592 | bytes 786432 | tf_op jit(solution)/shard_map/pallas_call | solution.py:274
  120.4 0.9 collective-permute-start.19
  121.2 2.4 %shard_map.143 = bf16[256,512]{1,0:T(8,128)(2,1)} custom-call(s32[1]{0:T(128)} %bitcast.14.at_ref, bf16[256,768]{1,0:T(8,128)(2,1)} %shard_map.140.x_ref, bf16[2048,2304]{1,0:T(8,128)(2,1)} %all-gather.2.cloned.1.call-done.gate_ref.up_ref.w_ref), custom_call_target="tpu_custom_call" | custom-call | flops 201326592 | bytes 786432 | tf_op jit(solution)/shard_map/pallas_call | solution.py:274
  123.6 3.2 %collective-permute-start.20 = (bf16[256,512]{1,0:T(8,128)(2,1)}, bf16[256,512]{1,0:T(8,128)(2,1)S(1)}, u32[]{:S(2)}, u32[]{:S(2)}) collective-permute-start(bf16[256,512]{1,0:T(8,128)(2,1)} %shard_map.143), channel_id=1, source_target_pairs={{0,2},{1,3},{2,0},{3,1},{4,6},{5,7},{6,4},{7,5},{8,10},{9,11},{10,... | collective-permute-start | bytes 786440 | tf_op jit(solution)/shard_map/ppermute | solution.py:219
  126.8 2.4 %shard_map.144 = bf16[256,512]{1,0:T(8,128)(2,1)} custom-call(s32[1]{0:T(128)} %bitcast.15.at_ref, bf16[256,768]{1,0:T(8,128)(2,1)} %shard_map.140.x_ref, bf16[2048,2304]{1,0:T(8,128)(2,1)} %all-gather.2.cloned.1.call-done.gate_ref.up_ref.w_ref), custom_call_target="tpu_custom_call" | custom-call | flops 201326592 | bytes 786432 | tf_op jit(solution)/shard_map/pallas_call | solution.py:274
  129.2 2.4 %shard_map.141 = bf16[256,512]{1,0:T(8,128)(2,1)} custom-call(s32[1]{0:T(128)} %bitcast.8.at_ref, bf16[256,768]{1,0:T(8,128)(2,1)} %shard_map.140.x_ref, bf16[2048,2304]{1,0:T(8,128)(2,1)} %all-gather.2.cloned.1.call-done.gate_ref.up_ref.w_ref), custom_call_target="tpu_custom_call" | custom-call | flops 201326592 | bytes 786432 | tf_op jit(solution)/shard_map/pallas_call | solution.py:274
  131.6 4.8 %collective-permute-done.20 = bf16[256,512]{1,0:T(8,128)(2,1)S(1)} collective-permute-done((bf16[256,512]{1,0:T(8,128)(2,1)}, bf16[256,512]{1,0:T(8,128)(2,1)S(1)}, u32[]{:S(2)}, u32[]{:S(2)}) %collective-permute-start.20) | collective-permute-done | bytes 262176 | tf_op jit(solution)/shard_map/ppermute | solution.py:219
  136.4 1.8 %collective-permute-done.21 = bf16[256,512]{1,0:T(8,128)(2,1)S(1)} collective-permute-done((bf16[256,512]{1,0:T(8,128)(2,1)}, bf16[256,512]{1,0:T(8,128)(2,1)S(1)}, u32[]{:S(2)}, u32[]{:S(2)}) %collective-permute-start.21) | collective-permute-done | bytes 262176 | tf_op jit(solution)/shard_map/ppermute | solution.py:219
  138.2 1.3 fusion.1
  139.5 1.0 collective-permute-start.22
  140.5 3.3 %collective-permute-start.23 = (f32[2,256]{1,0:T(2,128)S(1)}, f32[2,256]{1,0:T(2,128)S(1)}, u32[]{:S(2)}, u32[]{:S(2)}) collective-permute-start(f32[2,256]{1,0:T(2,128)S(1)} %pad_maximum_fusion.2), channel_id=1, source_target_pairs={{0,2},{1,3},{2,0},{3,1},{4,6},{5,7},{6,4},{7,5},{8,10},{9,11},{10,... | collective-permute-start | bytes 6152 | tf_op jit(solution)/shard_map/ppermute | solution.py:219
  144.5 1.1 collective-permute-done.23
  145.6 1.8 %collective-permute-done.24 = f32[2,256]{1,0:T(2,128)S(1)} collective-permute-done((f32[2,256]{1,0:T(2,128)S(1)}, f32[2,256]{1,0:T(2,128)S(1)}, u32[]{:S(2)}, u32[]{:S(2)}) %collective-permute-start.24) | collective-permute-done | bytes 2080 | tf_op jit(solution)/shard_map/ppermute | solution.py:219
  147.4 0.9 add_convert_fusion
  (64 shorter events, 5.9 us)
Async XLA Ops:
  6.5 63.5 %copy-start = (bf16[256,2048]{1,0:T(8,128)(2,1)S(1)}, bf16[256,2048]{1,0:T(8,128)(2,1)}, u32[]{:S(2)}) copy-start(bf16[256,2048]{1,0:T(8,128)(2,1)} %param.21) | copy-start | bytes 3145732
  6.6 104.4 %all-gather.2.cloned.1.call-start = ((), (), s32[]{:S(2)}) async-start(), calls=%async_computation | async-start | bytes 9732096 | tf_op jit(solution)/shard_map/all_gather | solution.py:295
  10.8 16.2 %collective-permute-start = (bf16[40,256]{1,0:T(8,128)(2,1)}, bf16[40,256]{1,0:T(8,128)(2,1)S(1)}, u32[]{:S(2)}, u32[]{:S(2)}) collective-permute-start(bf16[40,256]{1,0:T(8,128)(2,1)} %get-tuple-element.13), channel_id=1, source_target_pairs={{0,4},{4,8},{8,12},{12,16},{16,20},{20,24},{24,28},{28,32},{32,36}... | collective-permute-start | bytes 61448 | tf_op jit(solution)/shard_map/ppermute | solution.py:208
  12.6 16.5 %collective-permute-start.1 = (bf16[40,256]{1,0:T(8,128)(2,1)}, bf16[40,256]{1,0:T(8,128)(2,1)S(1)}, u32[]{:S(2)}, u32[]{:S(2)}) collective-permute-start(bf16[40,256]{1,0:T(8,128)(2,1)} %get-tuple-element.13), channel_id=1, source_target_pairs={{0,8},{4,12},{8,16},{12,20},{16,24},{20,28},{24,32},{28,36},{32,40... | collective-permute-start | bytes 61448 | tf_op jit(solution)/shard_map/ppermute | solution.py:208
  17.4 11.7 %collective-permute-start.2 = (bf16[40,256]{1,0:T(8,128)(2,1)}, bf16[40,256]{1,0:T(8,128)(2,1)S(1)}, u32[]{:S(2)}, u32[]{:S(2)}) collective-permute-start(bf16[40,256]{1,0:T(8,128)(2,1)} %get-tuple-element.13), channel_id=1, source_target_pairs={{0,12},{4,16},{8,20},{12,24},{16,28},{20,32},{24,36},{28,40},{32,4... | collective-permute-start | bytes 61448 | tf_op jit(solution)/shard_map/ppermute | solution.py:208
  24.4 4.8 %collective-permute-start.3 = (bf16[40,256]{1,0:T(8,128)(2,1)}, bf16[40,256]{1,0:T(8,128)(2,1)S(1)}, u32[]{:S(2)}, u32[]{:S(2)}) collective-permute-start(bf16[40,256]{1,0:T(8,128)(2,1)} %get-tuple-element.14), channel_id=1, source_target_pairs={{4,0},{8,4},{12,8},{16,12},{20,16},{24,20},{28,24},{32,28},{36,32}... | collective-permute-start | bytes 61448 | tf_op jit(solution)/shard_map/ppermute | solution.py:209
  25.7 8.6 %collective-permute-start.4 = (bf16[40,256]{1,0:T(8,128)(2,1)}, bf16[40,256]{1,0:T(8,128)(2,1)S(1)}, u32[]{:S(2)}, u32[]{:S(2)}) collective-permute-start(bf16[40,256]{1,0:T(8,128)(2,1)} %get-tuple-element.14), channel_id=1, source_target_pairs={{8,0},{12,4},{16,8},{20,12},{24,16},{28,20},{32,24},{36,28},{40,32... | collective-permute-start | bytes 61448 | tf_op jit(solution)/shard_map/ppermute | solution.py:209
  27.0 9.0 %copy-start.9 = (bf16[40,256]{1,0:T(8,128)(2,1)}, bf16[40,256]{1,0:T(8,128)(2,1)S(1)}, u32[]{:S(2)}) copy-start(bf16[40,256]{1,0:T(8,128)(2,1)S(1)} %collective-permute-done.f1) | copy-start | bytes 61444
  27.0 9.0 %collective-permute-start.5 = (bf16[40,256]{1,0:T(8,128)(2,1)}, bf16[40,256]{1,0:T(8,128)(2,1)S(1)}, u32[]{:S(2)}, u32[]{:S(2)}) collective-permute-start(bf16[40,256]{1,0:T(8,128)(2,1)} %get-tuple-element.14), channel_id=1, source_target_pairs={{12,0},{16,4},{20,8},{24,12},{28,16},{32,20},{36,24},{40,28},{44,3... | collective-permute-start | bytes 61448 | tf_op jit(solution)/shard_map/ppermute | solution.py:209
  29.1 6.8 %copy-start.10 = (bf16[40,256]{1,0:T(8,128)(2,1)}, bf16[40,256]{1,0:T(8,128)(2,1)S(1)}, u32[]{:S(2)}) copy-start(bf16[40,256]{1,0:T(8,128)(2,1)S(1)} %collective-permute-done.1.f2) | copy-start | bytes 61444
  29.2 6.8 %copy-start.11 = (bf16[40,256]{1,0:T(8,128)(2,1)}, bf16[40,256]{1,0:T(8,128)(2,1)S(1)}, u32[]{:S(2)}) copy-start(bf16[40,256]{1,0:T(8,128)(2,1)S(1)} %collective-permute-done.2.f3) | copy-start | bytes 61444
  29.2 6.8 %copy-start.12 = (bf16[40,256]{1,0:T(8,128)(2,1)}, bf16[40,256]{1,0:T(8,128)(2,1)S(1)}, u32[]{:S(2)}) copy-start(bf16[40,256]{1,0:T(8,128)(2,1)S(1)} %collective-permute-done.3.b1) | copy-start | bytes 61444
  34.2 1.8 %copy-start.13 = (bf16[40,256]{1,0:T(8,128)(2,1)}, bf16[40,256]{1,0:T(8,128)(2,1)S(1)}, u32[]{:S(2)}) copy-start(bf16[40,256]{1,0:T(8,128)(2,1)S(1)} %collective-permute-done.4.b2) | copy-start | bytes 61444
  36.0 0.6 copy-start.14
  38.3 24.1 %collective-permute-start.6 = (bf16[40,256]{1,0:T(8,128)(2,1)}, bf16[40,256]{1,0:T(8,128)(2,1)S(1)}, u32[]{:S(2)}, u32[]{:S(2)}) collective-permute-start(bf16[40,256]{1,0:T(8,128)(2,1)} %get-tuple-element.15.f1), channel_id=1, source_target_pairs={{0,12},{4,16},{8,20},{12,24},{16,28},{20,32},{24,36},{28,40},{32,4... | collective-permute-start | bytes 61448 | tf_op jit(solution)/shard_map/ppermute | solution.py:208
  44.9 17.5 %collective-permute-start.7 = (bf16[40,256]{1,0:T(8,128)(2,1)}, bf16[40,256]{1,0:T(8,128)(2,1)S(1)}, u32[]{:S(2)}, u32[]{:S(2)}) collective-permute-start(bf16[40,256]{1,0:T(8,128)(2,1)} %get-tuple-element.15.f1), channel_id=1, source_target_pairs={{0,24},{4,28},{8,32},{12,36},{16,40},{20,44},{24,48},{28,52},{32,5... | collective-permute-start | bytes 61448 | tf_op jit(solution)/shard_map/ppermute | solution.py:208
  55.0 7.4 %collective-permute-start.8 = (bf16[40,256]{1,0:T(8,128)(2,1)}, bf16[40,256]{1,0:T(8,128)(2,1)S(1)}, u32[]{:S(2)}, u32[]{:S(2)}) collective-permute-start(bf16[40,256]{1,0:T(8,128)(2,1)} %get-tuple-element.16.b1), channel_id=1, source_target_pairs={{12,0},{16,4},{20,8},{24,12},{28,16},{32,20},{36,24},{40,28},{44,3... | collective-permute-start | bytes 61448 | tf_op jit(solution)/shard_map/ppermute | solution.py:209
  56.3 10.7 %collective-permute-start.9 = (bf16[40,256]{1,0:T(8,128)(2,1)}, bf16[40,256]{1,0:T(8,128)(2,1)S(1)}, u32[]{:S(2)}, u32[]{:S(2)}) collective-permute-start(bf16[40,256]{1,0:T(8,128)(2,1)} %get-tuple-element.16.b1), channel_id=1, source_target_pairs={{24,0},{28,4},{32,8},{36,12},{40,16},{44,20},{48,24},{52,28},{56,3... | collective-permute-start | bytes 61448 | tf_op jit(solution)/shard_map/ppermute | solution.py:209
  62.4 4.7 %copy-start.5 = (bf16[40,256]{1,0:T(8,128)(2,1)}, bf16[40,256]{1,0:T(8,128)(2,1)S(1)}, u32[]{:S(2)}) copy-start(bf16[40,256]{1,0:T(8,128)(2,1)S(1)} %collective-permute-done.6.f2) | copy-start | bytes 61444
  62.4 4.7 %copy-start.6 = (bf16[40,256]{1,0:T(8,128)(2,1)}, bf16[40,256]{1,0:T(8,128)(2,1)S(1)}, u32[]{:S(2)}) copy-start(bf16[40,256]{1,0:T(8,128)(2,1)S(1)} %collective-permute-done.7.f3) | copy-start | bytes 61444
  62.4 4.6 %copy-start.7 = (bf16[40,256]{1,0:T(8,128)(2,1)}, bf16[40,256]{1,0:T(8,128)(2,1)S(1)}, u32[]{:S(2)}) copy-start(bf16[40,256]{1,0:T(8,128)(2,1)S(1)} %collective-permute-done.8.b2) | copy-start | bytes 61444
  67.0 0.6 copy-start.8
  71.5 9.6 %collective-permute-start.10 = (bf16[256,512]{1,0:T(8,128)(2,1)S(1)}, bf16[256,512]{1,0:T(8,128)(2,1)S(1)}, u32[]{:S(2)}, u32[]{:S(2)}) collective-permute-start(bf16[256,512]{1,0:T(8,128)(2,1)S(1)} %get-tuple-element.23), channel_id=1, source_target_pairs={{0,1},{1,2},{2,3},{3,0},{4,5},{5,6},{6,7},{7,4},{8,9},{9,10},{10,1... | collective-permute-start | bytes 786440 | tf_op jit(solution)/shard_map/ppermute | solution.py:219
  73.4 14.1 %collective-permute-start.11 = (bf16[256,512]{1,0:T(8,128)(2,1)S(1)}, bf16[256,512]{1,0:T(8,128)(2,1)S(1)}, u32[]{:S(2)}, u32[]{:S(2)}) collective-permute-start(bf16[256,512]{1,0:T(8,128)(2,1)S(1)} %get-tuple-element.25), channel_id=1, source_target_pairs={{0,2},{1,3},{2,0},{3,1},{4,6},{5,7},{6,4},{7,5},{8,10},{9,11},{10,... | collective-permute-start | bytes 786440 | tf_op jit(solution)/shard_map/ppermute | solution.py:219
  75.9 11.5 %collective-permute-start.12 = (bf16[256,512]{1,0:T(8,128)(2,1)S(1)}, bf16[256,512]{1,0:T(8,128)(2,1)S(1)}, u32[]{:S(2)}, u32[]{:S(2)}) collective-permute-start(bf16[256,512]{1,0:T(8,128)(2,1)S(1)} %get-tuple-element.24), channel_id=1, source_target_pairs={{0,3},{1,0},{2,1},{3,2},{4,7},{5,4},{6,5},{7,6},{8,11},{9,8},{10,9... | collective-permute-start | bytes 786440 | tf_op jit(solution)/shard_map/ppermute | solution.py:219
  88.7 5.7 %collective-permute-start.13 = (f32[2,256]{1,0:T(2,128)S(1)}, f32[2,256]{1,0:T(2,128)S(1)}, u32[]{:S(2)}, u32[]{:S(2)}) collective-permute-start(f32[2,256]{1,0:T(2,128)S(1)} %pad_maximum_fusion.1), channel_id=1, source_target_pairs={{0,1},{1,2},{2,3},{3,0},{4,5},{5,6},{6,7},{7,4},{8,9},{9,10},{10,1... | collective-permute-start | bytes 6152 | tf_op jit(solution)/shard_map/ppermute | solution.py:219
  90.2 5.1 %collective-permute-start.14 = (f32[2,256]{1,0:T(2,128)S(1)}, f32[2,256]{1,0:T(2,128)S(1)}, u32[]{:S(2)}, u32[]{:S(2)}) collective-permute-start(f32[2,256]{1,0:T(2,128)S(1)} %pad_maximum_fusion.1), channel_id=1, source_target_pairs={{0,2},{1,3},{2,0},{3,1},{4,6},{5,7},{6,4},{7,5},{8,10},{9,11},{10,... | collective-permute-start | bytes 6152 | tf_op jit(solution)/shard_map/ppermute | solution.py:219
  92.6 3.6 %collective-permute-start.15 = (f32[2,256]{1,0:T(2,128)S(1)}, f32[2,256]{1,0:T(2,128)S(1)}, u32[]{:S(2)}, u32[]{:S(2)}) collective-permute-start(f32[2,256]{1,0:T(2,128)S(1)} %pad_maximum_fusion.1), channel_id=1, source_target_pairs={{0,3},{1,0},{2,1},{3,2},{4,7},{5,4},{6,5},{7,6},{8,11},{9,8},{10,9... | collective-permute-start | bytes 6152 | tf_op jit(solution)/shard_map/ppermute | solution.py:219
  96.3 14.6 %copy-start.1 = (bf16[256,512]{1,0:T(8,128)(2,1)}, bf16[256,512]{1,0:T(8,128)(2,1)S(1)}, u32[]{:S(2)}) copy-start(bf16[256,512]{1,0:T(8,128)(2,1)S(1)} %fusion.x0) | copy-start | bytes 786436
  96.4 14.0 %collective-permute-start.16 = (bf16[256,512]{1,0:T(8,128)(2,1)S(1)}, bf16[256,512]{1,0:T(8,128)(2,1)S(1)}, u32[]{:S(2)}, u32[]{:S(2)}) collective-permute-start(bf16[256,512]{1,0:T(8,128)(2,1)S(1)} %fusion.x0), channel_id=1, source_target_pairs={{0,1},{1,2},{2,3},{3,0},{4,5},{5,6},{6,7},{7,4},{8,9},{9,10},{10,1... | collective-permute-start | bytes 786440 | tf_op jit(solution)/shard_map/ppermute | solution.py:219
  97.2 13.2 %collective-permute-start.17 = (bf16[256,512]{1,0:T(8,128)(2,1)S(1)}, bf16[256,512]{1,0:T(8,128)(2,1)S(1)}, u32[]{:S(2)}, u32[]{:S(2)}) collective-permute-start(bf16[256,512]{1,0:T(8,128)(2,1)S(1)} %fusion.x0), channel_id=1, source_target_pairs={{0,2},{1,3},{2,0},{3,1},{4,6},{5,7},{6,4},{7,5},{8,10},{9,11},{10,... | collective-permute-start | bytes 786440 | tf_op jit(solution)/shard_map/ppermute | solution.py:219
  101.0 9.9 %collective-permute-start.18 = (bf16[256,512]{1,0:T(8,128)(2,1)S(1)}, bf16[256,512]{1,0:T(8,128)(2,1)S(1)}, u32[]{:S(2)}, u32[]{:S(2)}) collective-permute-start(bf16[256,512]{1,0:T(8,128)(2,1)S(1)} %fusion.x0), channel_id=1, source_target_pairs={{0,3},{1,0},{2,1},{3,2},{4,7},{5,4},{6,5},{7,6},{8,11},{9,8},{10,9... | collective-permute-start | bytes 786440 | tf_op jit(solution)/shard_map/ppermute | solution.py:219
  110.3 0.7 copy-start.2
  110.3 0.8 copy-start.3
  110.9 0.7 copy-start.4
  120.4 11.3 %collective-permute-start.19 = (bf16[256,512]{1,0:T(8,128)(2,1)}, bf16[256,512]{1,0:T(8,128)(2,1)S(1)}, u32[]{:S(2)}, u32[]{:S(2)}) collective-permute-start(bf16[256,512]{1,0:T(8,128)(2,1)} %shard_map.142), channel_id=1, source_target_pairs={{0,1},{1,2},{2,3},{3,0},{4,5},{5,6},{6,7},{7,4},{8,9},{9,10},{10,1... | collective-permute-start | bytes 786440 | tf_op jit(solution)/shard_map/ppermute | solution.py:219
  123.6 12.8 %collective-permute-start.20 = (bf16[256,512]{1,0:T(8,128)(2,1)}, bf16[256,512]{1,0:T(8,128)(2,1)S(1)}, u32[]{:S(2)}, u32[]{:S(2)}) collective-permute-start(bf16[256,512]{1,0:T(8,128)(2,1)} %shard_map.143), channel_id=1, source_target_pairs={{0,2},{1,3},{2,0},{3,1},{4,6},{5,7},{6,4},{7,5},{8,10},{9,11},{10,... | collective-permute-start | bytes 786440 | tf_op jit(solution)/shard_map/ppermute | solution.py:219
  129.2 9.0 %collective-permute-start.21 = (bf16[256,512]{1,0:T(8,128)(2,1)}, bf16[256,512]{1,0:T(8,128)(2,1)S(1)}, u32[]{:S(2)}, u32[]{:S(2)}) collective-permute-start(bf16[256,512]{1,0:T(8,128)(2,1)} %shard_map.144), channel_id=1, source_target_pairs={{0,3},{1,0},{2,1},{3,2},{4,7},{5,4},{6,5},{7,6},{8,11},{9,8},{10,9... | collective-permute-start | bytes 786440 | tf_op jit(solution)/shard_map/ppermute | solution.py:219
  139.5 4.9 %collective-permute-start.22 = (f32[2,256]{1,0:T(2,128)S(1)}, f32[2,256]{1,0:T(2,128)S(1)}, u32[]{:S(2)}, u32[]{:S(2)}) collective-permute-start(f32[2,256]{1,0:T(2,128)S(1)} %pad_maximum_fusion.2), channel_id=1, source_target_pairs={{0,1},{1,2},{2,3},{3,0},{4,5},{5,6},{6,7},{7,4},{8,9},{9,10},{10,1... | collective-permute-start | bytes 6152 | tf_op jit(solution)/shard_map/ppermute | solution.py:219
  140.5 5.1 %collective-permute-start.23 = (f32[2,256]{1,0:T(2,128)S(1)}, f32[2,256]{1,0:T(2,128)S(1)}, u32[]{:S(2)}, u32[]{:S(2)}) collective-permute-start(f32[2,256]{1,0:T(2,128)S(1)} %pad_maximum_fusion.2), channel_id=1, source_target_pairs={{0,2},{1,3},{2,0},{3,1},{4,6},{5,7},{6,4},{7,5},{8,10},{9,11},{10,... | collective-permute-start | bytes 6152 | tf_op jit(solution)/shard_map/ppermute | solution.py:219
  143.8 3.6 %collective-permute-start.24 = (f32[2,256]{1,0:T(2,128)S(1)}, f32[2,256]{1,0:T(2,128)S(1)}, u32[]{:S(2)}, u32[]{:S(2)}) collective-permute-start(f32[2,256]{1,0:T(2,128)S(1)} %pad_maximum_fusion.2), channel_id=1, source_target_pairs={{0,3},{1,0},{2,1},{3,2},{4,7},{5,4},{6,5},{7,6},{8,11},{9,8},{10,9... | collective-permute-start | bytes 6152 | tf_op jit(solution)/shard_map/ppermute | solution.py:219
Sparse Core Ops, SparseCore 0:
  9.2 93.6 all-gather.1
